TPU v7x, 128 devices: a whole 4x4x4 slice. The times are simulated.
128 devices in a mesh: sp: 16 (over z, y), tp: 8 (over x, core).
Axes of the slice: x: 4, y: 4, z: 4, core: 2. Of those that a mesh axis runs over, the one named last changes fastest.
Arguments:
- query_proj: bfloat16 [16384, 2048], P('sp', 'tp'), may hold values from -6 to 6
- key_proj: bfloat16 [16384, 2048], P('sp', 'tp'), may hold values from -6 to 6
- value_proj: bfloat16 [16384, 4096], P('sp', 'tp'), may hold values from -6 to 6
- gate_proj: bfloat16 [16384, 4096], P('sp', 'tp'), may hold values from -6 to 6
- log_decay: float32 [16384, 8], P('sp', 'tp'), may hold values from -0.75 to 0, as said below
- residual: bfloat16 [16384, 2048], P('sp'), may hold values from -4 to 4
- out_weight: bfloat16 [4096, 2048], P('tp'), may hold values from -0.09375 to 0.09375
- norm_gain: float32 [2, 2048], replicated, may hold values from 0.1 to 1.9
- norm_bias: float32 [2, 2048], replicated, may hold values from -1.5 to 1.5
- up_gate: bfloat16 [2048, 5632], P('sp', 'tp'), may hold values from -0.125 to 0.125
- up_value: bfloat16 [2048, 5632], P('sp', 'tp'), may hold values from -0.125 to 0.125
- conv_weight: float32 [2, 3, 5632], P(None, None, 'tp'), may hold values from -3 to 3
- conv_bias: float32 [2, 5632], P(None, 'tp'), may hold values from -1.5 to 1.5
- down_weight: bfloat16 [5632, 2048], P('tp', 'sp'), may hold values from -0.078125 to 0.078125
Outputs:
- layer_output: bfloat16 [16384, 2048], P(('sp', 'tp'))
Inputs may be any that keep to these rules, and one draw needn't show every extreme that they name: `log_decay`: all entries are negative.
All inputs are finite; a program needn't handle non-finite values.
Results may differ from a plain program's by a relative error of at most 0.023.
Values may be sent and summed in bfloat16 or wider, within the bound.
No kernel may reach another device: no remote copies, remote signals or barrier semaphores. Data moves between devices by JAX's collectives and lax.ppermute only.
A program may use at most 128 MiB of HBM per device.

v0:
```python
import jax
import jax.numpy as jnp
from jax import lax
from jax.sharding import Mesh
from jax.sharding import PartitionSpec as P

BLOCK = 256
SP = ("sp_0", "sp_1")
SP_TP = ("sp_0", "sp_1", "tp")
alpha_scale = 8.0**0.25
rope_base = 10000.0
tiny_stabilizer = 1e-05


def turned_gather(arrays, axis, dims):
    turned = [jnp.moveaxis(a, dim, 0) for a, dim in zip(arrays, dims)]
    both = jnp.concatenate([t.reshape(len(t), -1) for t in turned], axis=1)
    out, at, finished = (lax.all_gather(both, axis, axis=0, tiled=True), 0, [])
    for t, dim in zip(turned, dims):
        piece = out[:, at : at + t[0].size].reshape(-1, *t.shape[1:])
        finished.append(jnp.moveaxis(piece, 0, dim))
        at += t[0].size
    return tuple(finished)


def neutral_like(x, identity):
    return jax.tree.map(
        lambda a, e: jnp.broadcast_to(jnp.asarray(e, a.dtype), a.shape), x, identity
    )


def entering(x, axes, combine, identity):
    before = start = neutral_like(x, identity)
    subtotal = x
    for axis in reversed(axes):
        length, position = (lax.axis_size(axis), lax.axis_index(axis))
        pieces = jax.tree.map(
            lambda part, kind: lax.all_gather(part.astype(kind), axis),
            subtotal,
            (jnp.bfloat16, jnp.bfloat16),
        )
        inside, subtotal = (start, start)
        for k in range(length):
            passed = k < position
            subtotal = combine(
                subtotal, jax.tree.map(lambda part, own: part[k].astype(own.dtype), pieces, x)
            )
            inside = jax.tree.map(lambda new, old: jnp.where(passed, new, old), subtotal, inside)
        before = combine(inside, before)
    return before


def passed_along(x, axis, by):
    length = lax.axis_size(axis)
    pairs = [(i, i + by) for i in range(length) if 0 <= i + by < length]
    return lax.ppermute(x, axis, pairs)


def rotate(vectors, positions):
    head_width = vectors.shape[-1]
    half_width = head_width // 2
    inverse_freq = rope_base ** (-2.0 * jnp.arange(half_width, dtype=jnp.float32) / head_width)
    angles = positions[:, None] * inverse_freq[None, :]
    cosine = jnp.cos(angles)[:, None, :]
    sine_part = jnp.sin(angles)[:, None, :]
    front = vectors[..., :half_width]
    second = vectors[..., half_width:]
    return jnp.concatenate(
        [front * cosine - second * sine_part, front * sine_part + second * cosine], axis=-1
    )


def layer_norm(values, gain, shift):
    average = values.mean(-1, keepdims=True)
    spread = jnp.square(values - average).mean(-1, keepdims=True)
    return (values - average) * lax.rsqrt(spread + tiny_stabilizer) * gain + shift


def block_parts(query_tile, lookup_piece, payload_piece, log_blk):
    cum_log = jnp.cumsum(log_blk, axis=0)
    cum_heads = cum_log.T
    log_gap = cum_heads[:, :, None] - cum_heads[:, None, :]
    offsets = jnp.arange(log_blk.shape[0])
    causal = (offsets[:, None] >= offsets[None, :])[None]
    weight = jnp.where(causal, jnp.exp(jnp.where(causal, log_gap, 0.0)), 0.0)
    score_matrix = jnp.einsum(
        "jka,ska->kjs", query_tile, lookup_piece, preferred_element_type=jnp.float32
    )
    segment_scaling = (score_matrix * weight).astype(jnp.bfloat16)
    within = jnp.einsum(
        "htm,mhe->the", segment_scaling, payload_piece, preferred_element_type=jnp.float32
    )
    block_total = cum_log[-1]
    to_end = jnp.exp(block_total[None, :] - cum_log)
    faded_lookup_vector = (lookup_piece.astype(jnp.float32) * to_end[:, :, None]).astype(
        jnp.bfloat16
    )
    summand_term = jnp.einsum(
        "ajo,ajd->jod", faded_lookup_vector, payload_piece, preferred_element_type=jnp.float32
    )
    scaled_query = (query_tile.astype(jnp.float32) * jnp.exp(cum_log)[:, :, None]).astype(
        jnp.bfloat16
    )
    return (within, scaled_query, summand_term, jnp.exp(block_total))


def causal_conv(rows, edge_rows, taps, shift):
    padded = jnp.concatenate([edge_rows, rows], axis=0).astype(jnp.float32)
    length = rows.shape[0]
    result = shift[None, :] + padded[0:length] * taps[0]
    result = result + padded[1 : length + 1] * taps[1]
    return result + padded[2 : length + 2] * taps[2]


def combine(earlier, later):
    return (earlier[0] * later[0], later[0][:, None, None] * earlier[1] + later[1])


def shards(
    query_proj,
    key_proj,
    value_proj,
    gate_proj,
    log_decay,
    residual,
    out_weight,
    norm_gain,
    norm_bias,
    up_gate,
    up_value,
    conv_weight,
    conv_bias,
    down_weight,
):
    tok_rows = query_proj.shape[0]
    head_count = log_decay.shape[1]
    key_width = query_proj.shape[1] // head_count
    value_width = value_proj.shape[1] // head_count
    full_gate, full_value, full_down = turned_gather(
        (up_gate, up_value, down_weight), SP, (0, 0, 1)
    )
    positions = (lax.axis_index(SP) * tok_rows + jnp.arange(tok_rows)).astype(jnp.float32)
    query_rot = rotate(
        query_proj.astype(jnp.float32).reshape(tok_rows, head_count, key_width), positions
    ).astype(jnp.bfloat16)
    key_rot = (
        rotate(key_proj.astype(jnp.float32).reshape(tok_rows, head_count, key_width), positions)
        * key_width ** (-0.5)
    ).astype(jnp.bfloat16)
    block_count = tok_rows // BLOCK
    asking_segments = query_rot.reshape(block_count, BLOCK, head_count, key_width)
    key_blocks = key_rot.reshape(block_count, BLOCK, head_count, key_width)
    value_blocks = value_proj.reshape(block_count, BLOCK, head_count, value_width)
    log_blocks = log_decay.reshape(block_count, BLOCK, head_count)
    within, scaled_query, summand_term, block_decay = jax.vmap(block_parts)(
        asking_segments, key_blocks, value_blocks, log_blocks
    )

    def absorb(carry_state, pieces):
        return (pieces[1][:, None, None] * carry_state + pieces[0], None)

    zero_state = jnp.zeros((head_count, key_width, value_width), jnp.float32)
    own_state, _ = lax.scan(absorb, zero_state, (summand_term, block_decay))
    own_decay = jnp.prod(block_decay, axis=0)
    _, incoming = entering(
        (own_decay, own_state), SP, combine, (jnp.ones_like(own_decay), zero_state)
    )

    def advance(carry_state, pieces):
        carried = jnp.einsum(
            "thd,hde->the",
            pieces[0],
            carry_state.astype(jnp.bfloat16),
            preferred_element_type=jnp.float32,
        )
        return (pieces[2][:, None, None] * carry_state + pieces[1], carried)

    _, carried = lax.scan(advance, incoming, (scaled_query, summand_term, block_decay))
    mixed_heads = (within + carried).reshape(tok_rows, head_count, value_width)
    average = mixed_heads.mean(-1, keepdims=True)
    spread = jnp.square(mixed_heads - average).mean(-1, keepdims=True)
    standardized_rows = (mixed_heads - average) * lax.rsqrt(spread + tiny_stabilizer)
    gate_heads = gate_proj.astype(jnp.float32).reshape(tok_rows, head_count, value_width)
    gated_rows = (
        (jax.nn.silu(gate_heads) * standardized_rows)
        .astype(jnp.bfloat16)
        .reshape(tok_rows, head_count * value_width)
    )
    own_count = tok_rows // lax.axis_size("tp")
    partial_rows = jnp.dot(gated_rows, out_weight, preferred_element_type=jnp.float32)
    attended = lax.psum_scatter(
        partial_rows.astype(jnp.bfloat16), "tp", scatter_dimension=0, tiled=True
    ).astype(jnp.float32)
    own_residual = lax.dynamic_slice_in_dim(
        residual, lax.axis_index("tp") * own_count, own_count, 0
    )
    normed_own = layer_norm(
        alpha_scale * own_residual.astype(jnp.float32) + attended, norm_gain[0], norm_bias[0]
    ).astype(jnp.bfloat16)
    whole_rows = lax.all_gather(normed_own, "tp", axis=0, tiled=True)
    gate_up = jnp.dot(whole_rows, full_gate, preferred_element_type=jnp.float32)
    value_up = jnp.dot(whole_rows, full_value, preferred_element_type=jnp.float32)
    gate_up = gate_up.astype(jnp.bfloat16)
    value_up = value_up.astype(jnp.bfloat16)
    edges = jnp.concatenate([gate_up[tok_rows - 2 :], value_up[tok_rows - 2 :]], axis=0)
    edges = passed_along(edges, SP, 1)
    gate_edge, value_edge = (edges[:2], edges[2:])
    gate_conv = causal_conv(gate_up, gate_edge, conv_weight[0], conv_bias[0])
    value_conv = causal_conv(value_up, value_edge, conv_weight[1], conv_bias[1])
    activated = (jax.nn.gelu(gate_conv) * value_conv).astype(jnp.bfloat16)
    partial_ffn = jnp.dot(activated, full_down, preferred_element_type=jnp.float32)
    ffn_out = lax.psum_scatter(
        partial_ffn.astype(jnp.bfloat16), "tp", scatter_dimension=0, tiled=True
    ).astype(jnp.float32)
    return layer_norm(
        alpha_scale * normed_own.astype(jnp.float32) + ffn_out, norm_gain[1], norm_bias[1]
    ).astype(jnp.bfloat16)


def solution(mesh):
    torus = Mesh(mesh.devices.reshape(4, 4, mesh.shape["tp"]), ("sp_0", "sp_1", "tp"))
    return jax.shard_map(
        shards,
        mesh=torus,
        in_specs=(
            P(SP, "tp"),
            P(SP, "tp"),
            P(SP, "tp"),
            P(SP, "tp"),
            P(SP, "tp"),
            P(SP, None),
            P("tp", None),
            P(),
            P(),
            P(SP, "tp"),
            P(SP, "tp"),
            P(None, None, "tp"),
            P(None, "tp"),
            P("tp", SP),
        ),
        out_specs=P(SP_TP, None),
        check_vma=False,
    )
```

profile of v0, /device:TPU:0, one launch (start us, length us, event | category | flops | bytes accessed | tf_op | source)
XLA Modules:
  0.0 314.5 jit_solution(11302256274251141249)
XLA Ops:
  7.4 2.4 reduce-window.6
  10.4 1.4 bitcast_convert_fusion
  11.8 3.1 fusion.56
  14.9 0.8 copy-done.3
  15.7 2.0 convolution_bitcast_fusion.1
  17.7 9.8 %while.24 = (s32[]{:T(128)}, f32[1,256,512]{2,1,0:T(8,128)S(1)}, f32[4,1]{0,1:T(1,128)S(1)}, f32[4,1,256,512]{3,2,1,0:T(8,128)}, s32[]{:T(128)}, /*index=5*/s32[]{:T(128)}) while((s32[]{:T(128)}, f32[1,256,512]{2,1,0:T(8,128)S(1)}, f32[4,1]{0,1:T(1,128)S(1)}, f32[4,1,256,512]{3,2,1,0:T(8,128)}, s32[]{:T(128)}, ...), condition=%wide.region_4.5_spmd.clone, body=%wide.region_3.4_spmd.clone.sunk | while | flops 393219 | bytes 1572971 | solution.py:163
  18.3 1.8 bitcast_add_fusion.8
  20.2 0.6 constant_dynamic-slice_fusion.5
  20.8 1.8 bitcast_add_fusion.8
  22.6 0.6 constant_dynamic-slice_fusion.5
  23.2 1.8 bitcast_add_fusion.8
  25.7 1.8 bitcast_add_fusion.8
  27.5 0.7 convert_element_type.303
  28.3 0.7 dynamic-slice
  29.0 0.7 exponential_reduce_fusion
  29.7 1.4 dynamic-update-slice
  31.0 10.8 %all-reduce = bf16[4]{0:T(256)(128)(2,1)S(1)} all-reduce(bf16[4]{0:T(256)(128)(2,1)S(1)} %dynamic-update-slice), channel_id=1, replica_groups=mesh['sp_0'=4,'sp_1'=4,'tp'=8] {'sp_1'}, use_global_device_ids=true, to_apply=%add | all-reduce | flops 4 | bytes 16
  41.9 0.7 slice_convert_fusion.3
  43.2 11.9 %all-gather.13.cloned.1.call-done = bf16[4,256,512]{2,1,0:T(8,128)(2,1)} async-done(((bf16[1,256,512]{2,1,0:T(8,128)(2,1)}), bf16[4,256,512]{2,1,0:T(8,128)(2,1)}) %all-gather.13.cloned.1.call-update) | async-done | bytes 1048592 | tf_op jit(solution)/shard_map/all_gather | solution.py:38
  55.0 4.0 %fusion.70 = bf16[1,1,256,512]{3,2,1,0:T(8,128)(2,1)} fusion(f32[]{:T(128)} %bitcast.39, f32[]{:T(128)} %bitcast.40, f32[]{:T(128)} %bitcast.41, f32[]{:T(128)} %bitcast.42, bf16[4,256,512]{2,1,0:T(8,128)(2,1)} %all-gather.13.cloned.1.call-done), kind=kLoop, calls=%fused_computation.102 | loop fusion | flops 1572864 | bytes 1310736 | tf_op jit(solution)/shard_map/convert_element_type | solution.py:38
  59.1 0.7 dynamic-slice.1
  59.7 0.6 fusion.101
  60.4 1.4 dynamic-update-slice.1
  61.8 10.7 %all-reduce.1 = bf16[4]{0:T(256)(128)(2,1)S(1)} all-reduce(bf16[4]{0:T(256)(128)(2,1)S(1)} %dynamic-update-slice.1), channel_id=2, replica_groups=mesh['sp_0'=4,'sp_1'=4,'tp'=8] {'sp_0'}, use_global_device_ids=true, to_apply=%add.1 | all-reduce | flops 4 | bytes 16
  72.5 0.7 fusion.100
  78.2 1.9 fusion.61
  80.2 3.6 %all-gather.7.cloned.1.call-done = bf16[4,1,256,512]{3,2,1,0:T(8,128)(2,1)} async-done(((bf16[1,1,256,512]{3,2,1,0:T(8,128)(2,1)}), bf16[4,1,256,512]{3,2,1,0:T(8,128)(2,1)}) %all-gather.7.cloned.1.call-update) | async-done | bytes 1048592 | tf_op jit(solution)/shard_map/all_gather | solution.py:38
  83.8 3.9 %fusion.69 = f32[1,256,512]{2,1,0:T(8,128)S(1)} fusion(bf16[4,1,256,512]{3,2,1,0:T(8,128)(2,1)} %all-gather.7.cloned.1.call-done, f32[]{:T(128)} %bitcast.39, f32[]{:T(128)} %bitcast.40, f32[]{:T(128)} %bitcast.41, f32[]{:T(128)} %bitcast.42, f32[]{:T(128)} %bitcast.33, f32[]{:T(128)S(6)} %convert.26, f32[]{:T(128)S(6)} %convert.27, f32[]{:T(128)} %bitcast.38, ...), kind=kLoop, calls=%fused_computation.99 | loop fusion | flops 4194304 | bytes 2621484 | tf_op jit(solution)/shard_map/add | solution.py:116
  87.7 17.8 %while.23 = (s32[]{:T(128)}, f32[1,256,512]{2,1,0:T(8,128)S(1)}, f32[4,256,1,512]{3,1,2,0:T(8,128)}, f32[4,1]{0,1:T(1,128)S(1)}, f32[4,1,256,512]{3,2,1,0:T(8,128)}, /*index=5*/bf16[4,256,1,256]{3,1,2,0:T(8,128)(2,1)}, s32[]{:T(128)}) while((s32[]{:T(128)}, f32[1,256,512]{2,1,0:T(8,128)S(1)}, f32[4,256,1,512]{3,1,2,0:T(8,128)}, ...), condition=%wide.region_6.7_spmd, body=%wide.region_5.6_spmd.sunk | while | flops 67502080 | bytes 2753641 | solution.py:178
  87.7 0.6 constant_dynamic-slice_fusion.4
  88.4 1.9 fusion.118
  90.3 1.9 bitcast_add_fusion.7
  92.2 0.6 constant_dynamic-slice_fusion.4
  92.8 1.9 fusion.118
  94.7 1.9 bitcast_add_fusion.7
  96.6 0.6 constant_dynamic-slice_fusion.4
  97.2 1.9 fusion.118
  99.2 1.9 bitcast_add_fusion.7
  101.1 0.6 constant_dynamic-slice_fusion.4
  101.7 1.9 fusion.118
  103.6 1.9 bitcast_add_fusion.7
  105.5 4.2 %fusion.102 = (f32[4,256]{1,0:T(4,128)S(1)}, f32[4,256,1,512]{3,1,0,2:T(8,128)}) fusion(f32[4,256,1,512]{3,1,2,0:T(8,128)} %get-tuple-element.60, bf16[4,256,512]{2,1,0:T(8,128)(2,1)} %bitcast.150, bf16[4,256,128]{2,1,0:T(8,128)(2,1)} %bitcast.155, bf16[4,256,128]{2,1,0:T(8,128)(2,1)S(1)} %bitcast.153, f32[4,256]{1,0:T(4,128)S(1)} %get-tuple-element.145, ...), kind=kOutput, calls=%fused_computation.160 | convolution fusion | flops 406846464 | bytes 6889472 | tf_op jit(solution)/shard_map/vmap(htm,mhe->the)/dot_general | solution.py:90
  109.8 2.1 multiply_reduce_fusion
  112.0 2.2 fusion.31
  114.2 4.3 %convolution_convert_fusion.1 = bf16[1024,2048]{1,0:T(8,128)(2,1)} fusion(bf16[1024,512]{1,0:T(8,128)(2,1)S(1)} %fusion.31, bf16[512,2048]{1,0:T(8,128)(2,1)S(1)} %copy-done), kind=kOutput, calls=%fused_computation.14 | convolution fusion | flops 2149580800 | bytes 7340032 | tf_op jit(solution)/shard_map/dot_general | solution.py:190
  118.6 0.8 copy-done.5
  119.6 0.9 pad_maximum_fusion
  120.6 36.8 %reduce-scatter.3.cloned.1.call-done = bf16[128,2048]{1,0:T(8,128)(2,1)} async-done(((bf16[1024,2048]{1,0:T(8,128)(2,1)}), bf16[128,2048]{1,0:T(8,128)(2,1)}) %reduce-scatter.3.cloned.1.call-update) | async-done | bytes 524304 | tf_op jit(solution)/shard_map/reduce_scatter | solution.py:191
  157.4 1.5 fusion.45
  158.9 1.6 multiply_reduce_fusion.2
  160.4 2.4 add_convert_fusion.1
  163.1 36.6 %all-gather.11.cloned.1.call-done = bf16[2048,2112]{0,1:T(8,128)(2,1)} async-done(((bf16[128,2112]{0,1:T(8,128)(2,1)}), bf16[2048,2112]{0,1:T(8,128)(2,1)}) %all-gather.11.cloned.1.call-update) | async-done | bytes 8650768 | tf_op jit(solution)/shard_map/all_gather | solution.py:18
  199.7 32.7 %all-gather.9.cloned.1.call-done = bf16[1024,2048]{1,0:T(8,128)(2,1)} async-done(((bf16[128,2048]{1,0:T(8,128)(2,1)}), bf16[1024,2048]{1,0:T(8,128)(2,1)}) %all-gather.9.cloned.1.call-update) | async-done | bytes 4194320 | tf_op jit(solution)/shard_map/all_gather | solution.py:200
  232.4 6.4 %fusion.32 = bf16[1024,704]{0,1:T(8,128)(2,1)S(1)} fusion(bf16[1024,2048]{1,0:T(8,128)(2,1)} %all-gather.9.cloned.1.call-done, bf16[2048,2112]{0,1:T(8,128)(2,1)} %all-gather.11.cloned.1.call-done), kind=kOutput, calls=%fused_computation.52 | convolution fusion | flops 2953510912 | bytes 8519680 | tf_op jit(solution)/shard_map/dot_general | solution.py:201
  239.0 5.0 %fusion.35 = bf16[1024,704]{0,1:T(8,128)(2,1)S(1)} fusion(bf16[1024,2048]{1,0:T(8,128)(2,1)S(1)} %copy-done.12, bf16[2048,2112]{0,1:T(8,128)(2,1)} %all-gather.11.cloned.1.call-done), kind=kOutput, calls=%fused_computation.53 | convolution fusion | flops 2953510912 | bytes 8519680 | tf_op jit(solution)/shard_map/dot_general | solution.py:202
  244.3 3.6 %collective-permute-start = (bf16[4,704]{0,1:T(8,128)(2,1)S(1)}, bf16[4,704]{0,1:T(8,128)(2,1)S(1)}, u32[]{:S(2)}, u32[]{:S(2)}) collective-permute-start(bf16[4,704]{0,1:T(8,128)(2,1)S(1)} %pad_maximum_fusion.1), channel_id=1, source_target_pairs={{0,8},{8,16},{16,24},{24,32},{32,40},{40,48},{48,56},{56,64},{64,7... | collective-permute-start | bytes 16904 | tf_op jit(solution)/shard_map/ppermute | solution.py:56
  247.9 3.9 %collective-permute-done = bf16[4,704]{0,1:T(8,128)(2,1)S(1)} collective-permute-done((bf16[4,704]{0,1:T(8,128)(2,1)S(1)}, bf16[4,704]{0,1:T(8,128)(2,1)S(1)}, u32[]{:S(2)}, u32[]{:S(2)}) %collective-permute-start) | collective-permute-done | bytes 5664 | tf_op jit(solution)/shard_map/ppermute | solution.py:56
  252.0 0.8 maximum_convert_fusion
  252.8 0.8 maximum_convert_fusion.1
  253.5 10.0 %convolution_convert_fusion = bf16[1024,2048]{1,0:T(8,128)(2,1)} fusion(bf16[2048,2112]{0,1:T(8,128)(2,1)} %all-gather.11.cloned.1.call-done, f32[1026,704]{0,1:T(8,128)S(1)} %maximum_convert_fusion.1, f32[1026,704]{0,1:T(8,128)S(1)} %maximum_convert_fusion, f32[704]{0:T(1024)S(1)} %get-tuple-element.120, f32[704]{0:T(1024)S(1)} %get-tuple-element.121, ...), kind=kOutput, calls=%fused_computation.13 | convolution fusion | flops 2970746880 | bytes 24412160 | tf_op jit(solution)/shard_map/dot_general | solution.py:211
  263.6 38.9 %reduce-scatter.5.cloned.1.call-done = bf16[128,2048]{1,0:T(8,128)(2,1)} async-done(((bf16[1024,2048]{1,0:T(8,128)(2,1)}), bf16[128,2048]{1,0:T(8,128)(2,1)}) %reduce-scatter.5.cloned.1.call-update) | async-done | bytes 524304 | tf_op jit(solution)/shard_map/reduce_scatter | solution.py:212
  302.5 1.3 fusion.46
  303.8 1.4 multiply_reduce_fusion.1
  305.2 2.2 add_convert_fusion
  (75 shorter events, 3.2 us)
Async XLA Ops:
  7.4 106.8 %copy-start = (bf16[512,2048]{1,0:T(8,128)(2,1)S(1)}, bf16[512,2048]{1,0:T(8,128)(2,1)}, u32[]{:S(2)}) copy-start(bf16[512,2048]{1,0:T(8,128)(2,1)} %param.24) | copy-start | bytes 6291460
  7.4 47.7 %all-gather.13.cloned.1.call-start = ((), (), s32[]{:S(2)}) async-start(), calls=%async_computation.7 | async-start | bytes 1310720 | tf_op jit(solution)/shard_map/all_gather | solution.py:38
  10.4 5.3 %copy-start.4 = (bf16[1024,512]{1,0:T(8,128)(2,1)S(1)}, bf16[1024,512]{1,0:T(8,128)(2,1)}, u32[]{:S(2)}) copy-start(bf16[1024,512]{1,0:T(8,128)(2,1)} %param.20) | copy-start | bytes 3145732
  14.9 0.8 copy-start.3
  17.7 10.6 %copy-start.14 = (u32[128]{0:T(128)S(1)}, u32[128]{0:T(128)}, u32[]{:S(2)}) copy-start(u32[128]{0:T(128)} %constant.99) | copy-start | bytes 1540
  17.7 41.3 %copy-start.13 = (u32[128]{0:T(128)S(1)}, u32[128]{0:T(128)}, u32[]{:S(2)}) copy-start(u32[128]{0:T(128)} %constant.104) | copy-start | bytes 1540
  28.3 55.6 %all-gather.7.cloned.1.call-start = ((), (), s32[]{:S(2)}) async-start(), calls=%async_computation.2 | async-start | bytes 1310720 | tf_op jit(solution)/shard_map/all_gather | solution.py:38
  59.0 98.4 %reduce-scatter.3.cloned.1.call-start = ((), (), s32[]{:S(2)}) async-start(), calls=%async_computation.3 | async-start | bytes 4718592 | tf_op jit(solution)/shard_map/reduce_scatter | solution.py:191
  109.7 2.2 copy-start.1
  118.5 0.9 copy-start.5
  118.5 1.0 copy-start.6
  118.5 1.1 copy-start.7
  118.5 2.1 copy-start.9
  118.5 2.1 copy-start.10
  118.5 81.2 %all-gather.11.cloned.1.call-start = ((), (), s32[]{:S(2)}) async-start(), calls=%async_computation.5 | async-start | bytes 9191424 | tf_op jit(solution)/shard_map/all_gather | solution.py:18
  119.6 43.5 %copy-start.8 = (f32[2,3,704]{2,0,1:T(2,128)S(1)}, f32[2,3,704]{2,0,1:T(2,128)}, u32[]{:S(2)}) copy-start(f32[2,3,704]{2,0,1:T(2,128)} %param.29) | copy-start | bytes 50692
  120.5 111.9 %all-gather.9.cloned.1.call-start = ((), (), s32[]{:S(2)}) async-start(), calls=%async_computation.4 | async-start | bytes 4718592 | tf_op jit(solution)/shard_map/all_gather | solution.py:200
  162.8 139.7 %reduce-scatter.5.cloned.1.call-start = ((), (), s32[]{:S(2)}) async-start(), calls=%async_computation.6 | async-start | bytes 4718592 | tf_op jit(solution)/shard_map/reduce_scatter | solution.py:212
  232.4 6.5 %copy-start.12 = (bf16[1024,2048]{1,0:T(8,128)(2,1)S(1)}, bf16[1024,2048]{1,0:T(8,128)(2,1)}, u32[]{:S(2)}) copy-start(bf16[1024,2048]{1,0:T(8,128)(2,1)} %all-gather.9.cloned.1.call-done) | copy-start | bytes 12582916
  239.0 8.9 %copy-start.11 = (f32[2,704]{1,0:T(2,128)S(1)}, f32[2,704]{1,0:T(2,128)}, u32[]{:S(2)}) copy-start(f32[2,704]{1,0:T(2,128)} %param.30) | copy-start | bytes 16900
  244.3 7.6 %collective-permute-start = (bf16[4,704]{0,1:T(8,128)(2,1)S(1)}, bf16[4,704]{0,1:T(8,128)(2,1)S(1)}, u32[]{:S(2)}, u32[]{:S(2)}) collective-permute-start(bf16[4,704]{0,1:T(8,128)(2,1)S(1)} %pad_maximum_fusion.1), channel_id=1, source_target_pairs={{0,8},{8,16},{16,24},{24,32},{32,40},{40,48},{48,56},{56,64},{64,7... | collective-permute-start | bytes 16904 | tf_op jit(solution)/shard_map/ppermute | solution.py:56
  263.5 39.0 %copy-start.2 = (bf16[128,2048]{1,0:T(8,128)(2,1)S(1)}, bf16[128,2048]{1,0:T(8,128)(2,1)}, u32[]{:S(2)}) copy-start(bf16[128,2048]{1,0:T(8,128)(2,1)} %add_convert_fusion.1) | copy-start | bytes 1572868
Sparse Core Ops, SparseCore 0:
  28.4 26.5 all-gather.12
  59.1 24.6 all-gather.6
  118.7 38.6 reduce-scatter.2
  263.7 38.7 reduce-scatter.4
Sparse Core Ops, SparseCore 1:
  121.1 78.5 all-gather.10
  201.3 31.1 all-gather.8
where the time goes:
time: 316 us; the launch traced here: 314 us
  waiting for transfers between devices  165 us (52%)
  other arithmetic  51.6 us (16%)
  matrix products  39.7 us (13%)
  blocking collectives  21.5 us (7%)
  between operations  20.6 us (7%)
  local copies, waits for them, and re-layouts  12.4 us (4%)
  starting transfers between devices  4.01 us (1%)
    reduce_scatter x1, waiting for transfers between devices, shards(): lax.psum_scatter(partial_ffn.astype(jnp.bfloat16), 'tp', scatter_dimensio...  38.9 us
    reduce_scatter x1, waiting for transfers between devices, shards(): lax.psum_scatter(partial_rows.astype(jnp.bfloat16), 'tp', scatter_dimensi...  36.8 us
    all_gather x1, waiting for transfers between devices, turned_gather(): out, at, finished = (lax.all_gather(both, axis, axis=0, tiled=True), 0, [])  36.6 us
    all_gather x1, waiting for transfers between devices, shards(): whole_rows = lax.all_gather(normed_own, 'tp', axis=0, tiled=True)  32.7 us
    unnamed x2, blocking collectives  21.5 us
    all_gather x2, waiting for transfers between devices, entering(): lax.all_gather(part.astype(kind), axis)  15.5 us
    dot_general x1, matrix products, shards(): jnp.dot(activated, full_down, preferred_element_type=jnp.float32)  10 us
    dot_general x4, matrix products, advance(): jnp.einsum('thd,hde->the', pieces[0], carry_state.astype(jnp.bfloat16), p...  7.74 us
  transfers between devices with their start and end apart: 7, of which 7 were waited for; matrix products, arithmetic and copies ran while one was open for 5% of the time, Pallas kernels for 0%

commit v1 on v0

--- a/solution.py
+++ b/solution.py
@@ -197,7 +197,9 @@
     normed_own = layer_norm(
         alpha_scale * own_residual.astype(jnp.float32) + attended, norm_gain[0], norm_bias[0]
     ).astype(jnp.bfloat16)
-    whole_rows = lax.all_gather(normed_own, "tp", axis=0, tiled=True)
+    whole_rows = jnp.concatenate(
+        lax.all_to_all(jnp.stack([normed_own] * lax.axis_size("tp")), "tp", 0, 0), axis=0
+    )
     gate_up = jnp.dot(whole_rows, full_gate, preferred_element_type=jnp.float32)
     value_up = jnp.dot(whole_rows, full_value, preferred_element_type=jnp.float32)
     gate_up = gate_up.astype(jnp.bfloat16)

time: 316 us -> 302 us (0.956)
  waiting for transfers between devices: 165 us -> 144 us
  starting transfers between devices: 4.01 us -> 8.19 us
    all_to_all x0 -> x1, waiting for transfers between devices: none -> 49.3 us  [shards(): lax.all_to_all(jnp.stack([normed_own] * lax.axis_size('tp')), 'tp', 0, 0)]
    all_gather x1, waiting for transfers between devices: 36.6 us -> 0.01 us  [turned_gather(): out, at, finished = (lax.all_gather(both, axis, axis=0, tiled=True), 0, [])]
    all_gather x1 -> x0, waiting for transfers between devices: 32.7 us -> none  [shards(): whole_rows = lax.all_gather(normed_own, 'tp', axis=0, tiled=True)]
    all_to_all x0 -> x1, starting transfers between devices: none -> 4.72 us  [shards(): lax.all_to_all(jnp.stack([normed_own] * lax.axis_size('tp')), 'tp', 0, 0)]
  transfers between devices with their start and end apart: 7 -> 7, of which waited for: 7 -> 6; matrix products, arithmetic and copies ran while one was open for 5% -> 6% of each run, Pallas kernels for 0% -> 0%
where the time goes in v1:
time: 302 us; the launch traced here: 301 us
  waiting for transfers between devices  144 us (48%)
  other arithmetic  50.8 us (17%)
  matrix products  40.8 us (14%)
  blocking collectives  21.5 us (7%)
  between operations  20.6 us (7%)
  local copies, waits for them, and re-layouts  14.9 us (5%)
  starting transfers between devices  8.19 us (3%)
    all_to_all x1, waiting for transfers between devices, shards(): lax.all_to_all(jnp.stack([normed_own] * lax.axis_size('tp')), 'tp', 0, 0)  49.3 us
    reduce_scatter x1, waiting for transfers between devices, shards(): lax.psum_scatter(partial_ffn.astype(jnp.bfloat16), 'tp', scatter_dimensio...  38.6 us
    reduce_scatter x1, waiting for transfers between devices, shards(): lax.psum_scatter(partial_rows.astype(jnp.bfloat16), 'tp', scatter_dimensi...  36.8 us
    unnamed x2, blocking collectives  21.5 us
    all_gather x2, waiting for transfers between devices, entering(): lax.all_gather(part.astype(kind), axis)  15.5 us
    dot_general x1, matrix products, shards(): jnp.dot(activated, full_down, preferred_element_type=jnp.float32)  9.99 us
    dot_general x4, matrix products, advance(): jnp.einsum('thd,hde->the', pieces[0], carry_state.astype(jnp.bfloat16), p...  7.74 us
    add x4, other arithmetic, advance(): return (pieces[2][:, None, None] * carry_state + pieces[1], carried)  7.52 us
  transfers between devices with their start and end apart: 7, of which 6 were waited for; matrix products, arithmetic and copies ran while one was open for 6% of the time, Pallas kernels for 0%

profile of v1, /device:TPU:0, one launch (start us, length us, event | category | flops | bytes accessed | tf_op | source)
XLA Modules:
  0.0 300.7 jit_solution(2947872717915264978)
XLA Ops:
  7.4 2.4 reduce-window.6
  10.4 1.4 bitcast_convert_fusion
  11.8 3.1 %fusion.56 = (bf16[1024,1,128]{2,0,1:T(8,128)(2,1)S(1)}, bf16[1024,1,128]{2,0,1:T(8,128)(2,1)}, f32[1024,1,128]{2,0,1:T(8,128)S(1)}, f32[1024,1,128]{2,0,1:T(8,128)S(1)}) fusion(f32[1024,1,256]{2,0,1:T(8,128)S(1)} %get-tuple-element.182, f32[128]{0:T(128)S(1)} %multiply_power_fusion, f32[1024]{0:T(1024)S(1)} %add_convert_fusion.2, ...), kind=kLoop, calls=%fused_computation.87 | loop fusion | flops 1966080 | bytes 3674624 | tf_op jit(solution)/shard_map/convert.17
  14.9 0.8 copy-done.2
  15.7 2.0 convolution_bitcast_fusion.1
  17.7 9.8 %while.24 = (s32[]{:T(128)}, f32[1,256,512]{2,1,0:T(8,128)S(1)}, f32[4,1]{0,1:T(1,128)S(1)}, f32[4,1,256,512]{3,2,1,0:T(8,128)}, s32[]{:T(128)}, /*index=5*/s32[]{:T(128)}) while((s32[]{:T(128)}, f32[1,256,512]{2,1,0:T(8,128)S(1)}, f32[4,1]{0,1:T(1,128)S(1)}, f32[4,1,256,512]{3,2,1,0:T(8,128)}, s32[]{:T(128)}, ...), condition=%wide.region_4.5_spmd.clone, body=%wide.region_3.4_spmd.clone.sunk | while | flops 393219 | bytes 1572971 | solution.py:163
  18.3 1.8 bitcast_add_fusion.8
  20.2 0.6 constant_dynamic-slice_fusion.5
  20.8 1.8 bitcast_add_fusion.8
  23.2 1.8 bitcast_add_fusion.8
  25.7 1.8 bitcast_add_fusion.8
  27.5 0.7 convert_element_type.303
  28.3 0.7 dynamic-slice
  29.0 0.7 exponential_reduce_fusion
  29.7 1.4 dynamic-update-slice
  31.0 10.8 %all-reduce = bf16[4]{0:T(256)(128)(2,1)S(1)} all-reduce(bf16[4]{0:T(256)(128)(2,1)S(1)} %dynamic-update-slice), channel_id=1, replica_groups=mesh['sp_0'=4,'sp_1'=4,'tp'=8] {'sp_1'}, use_global_device_ids=true, to_apply=%add | all-reduce | flops 4 | bytes 16
  41.9 0.7 slice_convert_fusion.3
  43.2 11.9 %all-gather.10.cloned.1.call-done = bf16[4,256,512]{2,1,0:T(8,128)(2,1)} async-done(((bf16[1,256,512]{2,1,0:T(8,128)(2,1)}), bf16[4,256,512]{2,1,0:T(8,128)(2,1)}) %all-gather.10.cloned.1.call-update) | async-done | bytes 1048592 | tf_op jit(solution)/shard_map/all_gather | solution.py:38
  55.0 4.0 %fusion.70 = bf16[1,1,256,512]{3,2,1,0:T(8,128)(2,1)} fusion(f32[]{:T(128)} %bitcast.39, f32[]{:T(128)} %bitcast.40, f32[]{:T(128)} %bitcast.41, f32[]{:T(128)} %bitcast.42, bf16[4,256,512]{2,1,0:T(8,128)(2,1)} %all-gather.10.cloned.1.call-done), kind=kLoop, calls=%fused_computation.102 | loop fusion | flops 1572864 | bytes 1310736 | tf_op jit(solution)/shard_map/convert_element_type | solution.py:38
  59.1 0.7 dynamic-slice.1
  59.7 0.6 fusion.101
  60.4 1.4 dynamic-update-slice.1
  61.8 10.7 %all-reduce.1 = bf16[4]{0:T(256)(128)(2,1)S(1)} all-reduce(bf16[4]{0:T(256)(128)(2,1)S(1)} %dynamic-update-slice.1), channel_id=2, replica_groups=mesh['sp_0'=4,'sp_1'=4,'tp'=8] {'sp_0'}, use_global_device_ids=true, to_apply=%add.1 | all-reduce | flops 4 | bytes 16
  72.5 0.7 fusion.100
  78.2 1.9 fusion.61
  80.2 3.6 %all-gather.6.cloned.1.call-done = bf16[4,1,256,512]{3,2,1,0:T(8,128)(2,1)} async-done(((bf16[1,1,256,512]{3,2,1,0:T(8,128)(2,1)}), bf16[4,1,256,512]{3,2,1,0:T(8,128)(2,1)}) %all-gather.6.cloned.1.call-update) | async-done | bytes 1048592 | tf_op jit(solution)/shard_map/all_gather | solution.py:38
  83.8 3.9 %fusion.69 = f32[1,256,512]{2,1,0:T(8,128)S(1)} fusion(bf16[4,1,256,512]{3,2,1,0:T(8,128)(2,1)} %all-gather.6.cloned.1.call-done, f32[]{:T(128)} %bitcast.39, f32[]{:T(128)} %bitcast.40, f32[]{:T(128)} %bitcast.41, f32[]{:T(128)} %bitcast.42, f32[]{:T(128)} %bitcast.33, f32[]{:T(128)S(6)} %convert.26, f32[]{:T(128)S(6)} %convert.27, f32[]{:T(128)} %bitcast.38, ...), kind=kLoop, calls=%fused_computation.99 | loop fusion | flops 4194304 | bytes 2621484 | tf_op jit(solution)/shard_map/add | solution.py:116
  87.7 17.8 %while.23 = (s32[]{:T(128)}, f32[1,256,512]{2,1,0:T(8,128)S(1)}, f32[4,256,1,512]{3,1,2,0:T(8,128)}, f32[4,1]{0,1:T(1,128)S(1)}, f32[4,1,256,512]{3,2,1,0:T(8,128)}, /*index=5*/bf16[4,256,1,256]{3,1,2,0:T(8,128)(2,1)}, s32[]{:T(128)}) while((s32[]{:T(128)}, f32[1,256,512]{2,1,0:T(8,128)S(1)}, f32[4,256,1,512]{3,1,2,0:T(8,128)}, ...), condition=%wide.region_6.7_spmd, body=%wide.region_5.6_spmd.sunk | while | flops 67502080 | bytes 2753641 | solution.py:178
  87.7 0.6 constant_dynamic-slice_fusion.4
  88.4 1.9 fusion.118
  90.3 1.9 bitcast_add_fusion.7
  92.2 0.6 constant_dynamic-slice_fusion.4
  92.8 1.9 fusion.118
  94.7 1.9 bitcast_add_fusion.7
  96.6 0.6 constant_dynamic-slice_fusion.4
  97.2 1.9 fusion.118
  99.2 1.9 bitcast_add_fusion.7
  101.1 0.6 constant_dynamic-slice_fusion.4
  101.7 1.9 fusion.118
  103.6 1.9 bitcast_add_fusion.7
  105.5 4.2 %fusion.102 = (f32[4,256]{1,0:T(4,128)S(1)}, f32[4,256,1,512]{3,1,0,2:T(8,128)}) fusion(f32[4,256,1,512]{3,1,2,0:T(8,128)} %get-tuple-element.60, bf16[4,256,512]{2,1,0:T(8,128)(2,1)} %bitcast.151, bf16[4,256,128]{2,1,0:T(8,128)(2,1)} %bitcast.156, bf16[4,256,128]{2,1,0:T(8,128)(2,1)S(1)} %bitcast.154, f32[4,256]{1,0:T(4,128)S(1)} %get-tuple-element.145, ...), kind=kOutput, calls=%fused_computation.160 | convolution fusion | flops 406846464 | bytes 6889472 | tf_op jit(solution)/shard_map/vmap(htm,mhe->the)/dot_general | solution.py:90
  109.8 2.1 multiply_reduce_fusion
  112.0 2.2 fusion.31
  114.2 4.3 %convolution_convert_fusion.1 = bf16[1024,2048]{1,0:T(8,128)(2,1)} fusion(bf16[1024,512]{1,0:T(8,128)(2,1)S(1)} %fusion.31, bf16[512,2048]{1,0:T(8,128)(2,1)S(1)} %copy-done), kind=kOutput, calls=%fused_computation.14 | convolution fusion | flops 2149580800 | bytes 7340032 | tf_op jit(solution)/shard_map/dot_general | solution.py:190
  118.6 0.8 copy-done.4
  119.6 0.8 pad_maximum_fusion
  120.5 36.8 %reduce-scatter.3.cloned.1.call-done = bf16[128,2048]{1,0:T(8,128)(2,1)} async-done(((bf16[1024,2048]{1,0:T(8,128)(2,1)}), bf16[128,2048]{1,0:T(8,128)(2,1)}) %reduce-scatter.3.cloned.1.call-update) | async-done | bytes 524304 | tf_op jit(solution)/shard_map/reduce_scatter | solution.py:191
  157.4 1.5 fusion.45
  158.9 1.6 multiply_reduce_fusion.2
  160.4 1.6 add_convert_fusion.1
  162.0 2.5 stack.2
  164.5 4.7 %all-to-all-start = ((bf16[8,128,2048]{2,1,0:T(8,128)(2,1)}), bf16[8,128,2048]{2,1,0:T(8,128)(2,1)}, u32[]{:S(2)}, u32[]{:S(2)}) async-start(bf16[8,128,2048]{2,1,0:T(8,128)(2,1)} %stack.2), calls=%async_computation.1 | async-start | bytes 8388608 | tf_op jit(solution)/shard_map/all_to_all | solution.py:201
  169.5 49.3 %all-to-all-done = bf16[8,128,2048]{2,1,0:T(8,128)(2,1)} async-done(((bf16[8,128,2048]{2,1,0:T(8,128)(2,1)}), bf16[8,128,2048]{2,1,0:T(8,128)(2,1)}, u32[]{:S(2)}, u32[]{:S(2)}) %all-to-all-start) | async-done | bytes 4194336 | tf_op jit(solution)/shard_map/all_to_all | solution.py:201
  218.9 6.3 %fusion.32 = bf16[1024,704]{0,1:T(8,128)(2,1)S(1)} fusion(bf16[1024,2048]{1,0:T(8,128)(2,1)} %bitcast.59, bf16[2048,2112]{0,1:T(8,128)(2,1)} %all-gather.8.cloned.1.call-done), kind=kOutput, calls=%fused_computation.52 | convolution fusion | flops 2953510912 | bytes 8519680 | tf_op jit(solution)/shard_map/dot_general | solution.py:203
  225.3 6.3 %fusion.35 = bf16[1024,704]{0,1:T(8,128)(2,1)S(1)} fusion(bf16[1024,2048]{1,0:T(8,128)(2,1)} %bitcast.59, bf16[2048,2112]{0,1:T(8,128)(2,1)} %all-gather.8.cloned.1.call-done), kind=kOutput, calls=%fused_computation.53 | convolution fusion | flops 2953510912 | bytes 8519680 | tf_op jit(solution)/shard_map/dot_general | solution.py:204
  231.8 3.1 %collective-permute-start = (bf16[4,704]{0,1:T(8,128)(2,1)S(1)}, bf16[4,704]{0,1:T(8,128)(2,1)S(1)}, u32[]{:S(2)}, u32[]{:S(2)}) collective-permute-start(bf16[4,704]{0,1:T(8,128)(2,1)S(1)} %pad_maximum_fusion.1), channel_id=1, source_target_pairs={{0,8},{8,16},{16,24},{24,32},{32,40},{40,48},{48,56},{56,64},{64,7... | collective-permute-start | bytes 16904 | tf_op jit(solution)/shard_map/ppermute | solution.py:56
  235.0 3.5 %collective-permute-done = bf16[4,704]{0,1:T(8,128)(2,1)S(1)} collective-permute-done((bf16[4,704]{0,1:T(8,128)(2,1)S(1)}, bf16[4,704]{0,1:T(8,128)(2,1)S(1)}, u32[]{:S(2)}, u32[]{:S(2)}) %collective-permute-start) | collective-permute-done | bytes 5664 | tf_op jit(solution)/shard_map/ppermute | solution.py:56
  238.5 0.8 maximum_convert_fusion
  239.3 0.8 maximum_convert_fusion.1
  240.1 10.0 %convolution_convert_fusion = bf16[1024,2048]{1,0:T(8,128)(2,1)} fusion(bf16[2048,2112]{0,1:T(8,128)(2,1)} %all-gather.8.cloned.1.call-done, f32[1026,704]{0,1:T(8,128)S(1)} %maximum_convert_fusion.1, f32[1026,704]{0,1:T(8,128)S(1)} %maximum_convert_fusion, f32[704]{0:T(1024)S(1)} %get-tuple-element.120, f32[704]{0:T(1024)S(1)} %get-tuple-element.121, ...), kind=kOutput, calls=%fused_computation.13 | convolution fusion | flops 2970746880 | bytes 24412160 | tf_op jit(solution)/shard_map/dot_general | solution.py:213
  250.1 38.6 %reduce-scatter.5.cloned.1.call-done = bf16[128,2048]{1,0:T(8,128)(2,1)} async-done(((bf16[1024,2048]{1,0:T(8,128)(2,1)}), bf16[128,2048]{1,0:T(8,128)(2,1)}) %reduce-scatter.5.cloned.1.call-update) | async-done | bytes 524304 | tf_op jit(solution)/shard_map/reduce_scatter | solution.py:214
  288.7 1.3 fusion.46
  290.0 1.4 multiply_reduce_fusion.1
  291.4 2.2 add_convert_fusion
  (71 shorter events, 3.7 us)
Async XLA Ops:
  7.4 106.8 %copy-start = (bf16[512,2048]{1,0:T(8,128)(2,1)S(1)}, bf16[512,2048]{1,0:T(8,128)(2,1)}, u32[]{:S(2)}) copy-start(bf16[512,2048]{1,0:T(8,128)(2,1)} %param.24) | copy-start | bytes 6291460
  7.4 47.7 %all-gather.10.cloned.1.call-start = ((), (), s32[]{:S(2)}) async-start(), calls=%async_computation.7 | async-start | bytes 1310720 | tf_op jit(solution)/shard_map/all_gather | solution.py:38
  10.4 5.3 %copy-start.3 = (bf16[1024,512]{1,0:T(8,128)(2,1)S(1)}, bf16[1024,512]{1,0:T(8,128)(2,1)}, u32[]{:S(2)}) copy-start(bf16[1024,512]{1,0:T(8,128)(2,1)} %param.20) | copy-start | bytes 3145732
  14.9 0.8 copy-start.2
  17.7 10.6 %copy-start.12 = (u32[128]{0:T(128)S(1)}, u32[128]{0:T(128)}, u32[]{:S(2)}) copy-start(u32[128]{0:T(128)} %constant.99) | copy-start | bytes 1540
  17.7 41.3 %copy-start.11 = (u32[128]{0:T(128)S(1)}, u32[128]{0:T(128)}, u32[]{:S(2)}) copy-start(u32[128]{0:T(128)} %constant.104) | copy-start | bytes 1540
  28.3 55.6 %all-gather.6.cloned.1.call-start = ((), (), s32[]{:S(2)}) async-start(), calls=%async_computation.3 | async-start | bytes 1310720 | tf_op jit(solution)/shard_map/all_gather | solution.py:38
  59.0 98.4 %reduce-scatter.3.cloned.1.call-start = ((), (), s32[]{:S(2)}) async-start(), calls=%async_computation.4 | async-start | bytes 4718592 | tf_op jit(solution)/shard_map/reduce_scatter | solution.py:191
  109.7 2.2 copy-start.1
  118.5 0.9 copy-start.4
  118.5 1.0 copy-start.5
  118.5 1.1 copy-start.6
  118.5 2.0 copy-start.8
  118.5 2.0 copy-start.9
  118.5 100.3 %all-gather.8.cloned.1.call-start = ((), (), s32[]{:S(2)}) async-start(), calls=%async_computation.5 | async-start | bytes 9191424 | tf_op jit(solution)/shard_map/all_gather | solution.py:18
  164.5 5.0 %copy-start.7 = (f32[2,3,704]{2,0,1:T(2,128)S(1)}, f32[2,3,704]{2,0,1:T(2,128)}, u32[]{:S(2)}) copy-start(f32[2,3,704]{2,0,1:T(2,128)} %param.29) | copy-start | bytes 50692
  164.5 54.4 %all-to-all-start = ((bf16[8,128,2048]{2,1,0:T(8,128)(2,1)}), bf16[8,128,2048]{2,1,0:T(8,128)(2,1)}, u32[]{:S(2)}, u32[]{:S(2)}) async-start(bf16[8,128,2048]{2,1,0:T(8,128)(2,1)} %stack.2), calls=%async_computation.1 | async-start | bytes 8388608 | tf_op jit(solution)/shard_map/all_to_all | solution.py:201
  169.2 119.5 %reduce-scatter.5.cloned.1.call-start = ((), (), s32[]{:S(2)}) async-start(), calls=%async_computation.6 | async-start | bytes 4718592 | tf_op jit(solution)/shard_map/reduce_scatter | solution.py:214
  225.3 9.7 %copy-start.10 = (f32[2,704]{1,0:T(2,128)S(1)}, f32[2,704]{1,0:T(2,128)}, u32[]{:S(2)}) copy-start(f32[2,704]{1,0:T(2,128)} %param.30) | copy-start | bytes 16900
  231.8 6.6 %collective-permute-start = (bf16[4,704]{0,1:T(8,128)(2,1)S(1)}, bf16[4,704]{0,1:T(8,128)(2,1)S(1)}, u32[]{:S(2)}, u32[]{:S(2)}) collective-permute-start(bf16[4,704]{0,1:T(8,128)(2,1)S(1)} %pad_maximum_fusion.1), channel_id=1, source_target_pairs={{0,8},{8,16},{16,24},{24,32},{32,40},{40,48},{48,56},{56,64},{64,7... | collective-permute-start | bytes 16904 | tf_op jit(solution)/shard_map/ppermute | solution.py:56
Sparse Core Ops, SparseCore 0:
  28.4 26.5 all-gather.9
  59.1 24.6 all-gather.5
  118.7 38.6 reduce-scatter.2
  250.2 38.4 reduce-scatter.4
Sparse Core Ops, SparseCore 1:
  121.1 78.5 all-gather.7
